TPU v7x, 32 devices: a whole 2x2x4 slice. The times are simulated.
32 devices in a mesh: grp: 2 (over y), sp: 4 (over z), tp: 4 (over x, core).
Axes of the slice: x: 2, y: 2, z: 4, core: 2. Of those that a mesh axis runs over, the one named last changes fastest.
Arguments:
- tokens: bfloat16 [3072, 2048], P(('grp', 'sp')), parts along dimension 0, may hold values from -6 to 6
- norm_gain: float32 [2, 2048], replicated, may hold values from 0.1 to 1.9
- entry_weight: bfloat16 [2, 2048, 2048], P(None, 'sp', 'tp'), may hold values from -0.125 to 0.125
- mix_weight: bfloat16 [2, 4, 512, 512], P(None, 'tp'), may hold values from -0.25 to 0.25
- pool_gain: float32 [2, 2048], P(None, 'tp'), may hold values from 0.1 to 1.9
- back_weight: bfloat16 [2, 2048, 2048], P(None, 'tp', 'sp'), may hold values from -0.25 to 0.25
Outputs:
- result_tokens: bfloat16 [3072, 2048], P(('grp', 'sp')), parts along dimension 0
There are 2 independent parts, one for each index of `grp`. A program takes and returns all parts, laid end to end along the dimension named above; an argument that names none is the same for every part. Nothing has to cross between parts.
All inputs are finite; a program needn't handle non-finite values.
Results may differ from a plain program's by a relative error of at most 0.018.
Values may be sent and summed in bfloat16 or wider, within the bound.
A program may use at most 64 MiB of HBM per device.

v0:
```python
import jax
import jax.numpy as jnp
from jax import lax
from jax.sharding import PartitionSpec as P

GROUPS = 4
LAYERS = 2
EPSILON = 1e-05


def extended_2(value, sides, width):
    for axis, dim in sides:
        size, length = (lax.axis_size(axis), value.shape[dim])
        up = [(i, (i + 1) % size) for i in range(size - 1)]
        down = [(j, i) for i, j in up]
        last = lax.slice_in_dim(value, length - width, length, axis=dim)
        first = lax.slice_in_dim(value, 0, width, axis=dim)
        before = lax.ppermute(last, axis, up)
        after = lax.ppermute(first, axis, down)
        value = jnp.concatenate([before, value, after], axis=dim)
    return value


def window_mean(padded, positions, halves, total_length, reach):
    row_count = positions.shape[0]
    summed = jnp.zeros((row_count,) + padded.shape[1:], jnp.float32)
    for offset in range(-reach, reach):
        inside = ((offset >= -halves) & (offset < halves)).astype(jnp.float32)
        summed = (
            summed + padded[reach + offset : reach + offset + row_count] * inside[None, :, None]
        )
    lower = jnp.maximum(positions[:, None] - halves[None, :], 0)
    upper = jnp.minimum(positions[:, None] + halves[None, :], total_length)
    counted = (upper - lower).astype(jnp.float32)
    return summed / counted[:, :, None]


def normalize(state, gain):
    values = state.astype(jnp.float32)
    scaled = values * lax.rsqrt(jnp.mean(values * values, axis=-1, keepdims=True) + EPSILON)
    return (scaled * gain).astype(jnp.bfloat16)


def pool_groups(pooled_in, mix_layer, gain_layer, reach):
    row_count = pooled_in.shape[0]
    group_here = mix_layer.shape[0]
    width = mix_layer.shape[1]
    extended = extended_2(pooled_in, (("sp", 0),), reach)
    first_group = lax.axis_index("tp") * group_here
    halves = jnp.left_shift(jnp.int32(1), first_group + jnp.arange(group_here, dtype=jnp.int32))
    positions = lax.axis_index("sp") * row_count + jnp.arange(row_count, dtype=jnp.int32)
    total_length = lax.axis_size("sp") * row_count
    padded = extended.reshape(row_count + 2 * reach, group_here, width).astype(jnp.float32)
    means = window_mean(padded, positions, halves, total_length, reach)
    differ = (means - padded[reach : reach + row_count]).astype(jnp.bfloat16)
    mixed = jnp.einsum("tgc,gcd->tgd", differ, mix_layer, preferred_element_type=jnp.float32)
    return (mixed.reshape(row_count, group_here * width) * gain_layer).astype(jnp.bfloat16)


def per_device(tokens, norm_gain, entry_weight, mix_weight, pool_gain, back_weight):
    reach = 2 ** (GROUPS - 1)
    state = tokens
    entry_all, back_all = (
        lax.all_gather(entry_weight, "sp", axis=1, tiled=True),
        lax.all_gather(back_weight, "sp", axis=2, tiled=True),
    )
    for layer in range(LAYERS):
        normed = normalize(state, norm_gain[layer])
        pooled_in = jnp.dot(normed, entry_all[layer], preferred_element_type=jnp.float32).astype(
            jnp.bfloat16
        )
        back_local = back_all[layer]
        mixed = pool_groups(pooled_in, mix_weight[layer], pool_gain[layer], reach)
        update = jnp.dot(mixed, back_local, preferred_element_type=jnp.float32)
        summed = lax.psum(update.astype(jnp.bfloat16), "tp").astype(jnp.float32)
        state = (state.astype(jnp.float32) + summed).astype(jnp.bfloat16)
    return state


def solution(mesh):
    return jax.shard_map(
        per_device,
        mesh=mesh,
        in_specs=(
            P(("grp", "sp"), None),
            P(),
            P(None, "sp", "tp"),
            P(None, "tp", None, None),
            P(None, "tp"),
            P(None, "tp", "sp"),
        ),
        out_specs=P(("grp", "sp"), None),
        check_vma=False,
    )
```

profile of v0, /device:TPU:0, one launch (start us, length us, event | category | flops | bytes accessed | tf_op | source)
XLA Modules:
  0.0 298.0 jit_solution(13952838582287595426)
XLA Ops:
  6.5 0.0 copy-start
  6.5 0.0 copy-start.3
  6.5 0.0 copy-start.2
  6.5 0.0 all-gather.3.cloned.1.call-start
  6.5 0.7 all-gather.3.cloned.1.call-update
  7.3 0.0 all-gather.5.cloned.1.call-start
  7.3 0.7 all-gather.5.cloned.1.call-update
  8.0 0.0 all-reduce.3.cloned.1.call-start
  8.1 0.0 copy-done
  8.1 0.4 fusion
  8.5 0.0 copy-done.3
  8.5 0.0 copy-done.2
  8.5 83.9 %all-gather.3.cloned.1.call-done = bf16[2,2048,512]{2,1,0:T(8,128)(2,1)} async-done(((bf16[2,512,512]{2,1,0:T(8,128)(2,1)}), bf16[2,2048,512]{2,1,0:T(8,128)(2,1)}) %all-gather.3.cloned.1.call-update) | async-done | bytes 4194320 | tf_op jit(solution)/shard_map/all_gather | solution.py:64
  92.4 2.6 fusion.20
  95.0 1.3 collective-permute-start
  96.3 1.3 collective-permute-start.1
  97.8 0.0 collective-permute-done
  97.8 4.2 %collective-permute-done.1 = bf16[8,512]{1,0:T(8,128)(2,1)S(1)} collective-permute-done((bf16[8,512]{1,0:T(8,128)(2,1)S(1)}, bf16[8,512]{1,0:T(8,128)(2,1)S(1)}, u32[]{:S(2)}, u32[]{:S(2)}) %collective-permute-start.1) | collective-permute-done | bytes 8224 | tf_op jit(solution)/shard_map/ppermute | solution.py:19
  101.9 0.1 maximum_convert_fusion
  102.0 71.2 %all-gather.5.cloned.1.call-done = bf16[2,512,2048]{2,1,0:T(8,128)(2,1)} async-done(((bf16[2,512,512]{2,1,0:T(8,128)(2,1)}), bf16[2,512,2048]{2,1,0:T(8,128)(2,1)}) %all-gather.5.cloned.1.call-update) | async-done | bytes 4194320 | tf_op jit(solution)/shard_map/all_gather | solution.py:65
  173.2 5.3 %convolution_convert_fusion.1 = bf16[384,2048]{1,0:T(8,128)(2,1)} fusion(bf16[2,512,2048]{2,1,0:T(8,128)(2,1)} %all-gather.5.cloned.1.call-done, bf16[2,1,512,512]{3,2,1,0:T(8,128)(2,1)} %param.9, f32[512]{0:T(512)S(1)} %bitcast.87, f32[400,1,512]{2,0,1:T(8,128)S(1)} %maximum_convert_fusion, f32[384]{0:T(512)S(1)} %subtract_convert_fusion, f32[]{:T(128)S(6)} %mul.373, ...), kind=kOutput, calls=%fused_computation.15 | convolution fusion | flops 1014497280 | bytes 16781376 | tf_op jit(solution)/shard_map/dot_general | solution.py:74
  178.5 0.0 all-reduce.3.cloned.1.call-update
  178.5 0.0 all-reduce.5.cloned.1.call-start
  178.6 41.4 %all-reduce.3.cloned.1.call-done = bf16[384,2048]{1,0:T(8,128)(2,1)} async-done(((bf16[384,2048]{1,0:T(8,128)(2,1)}), bf16[384,2048]{1,0:T(8,128)(2,1)}) %all-reduce.3.cloned.1.call-update) | async-done | bytes 1572880 | tf_op jit(solution)/shard_map/psum | solution.py:75
  220.0 0.0 copy-start.1
  220.0 2.1 fusion.4
  222.1 0.0 copy-done.1
  222.1 2.6 fusion.23
  224.8 3.4 %collective-permute-start.2 = (bf16[8,512]{1,0:T(8,128)(2,1)S(1)}, bf16[8,512]{1,0:T(8,128)(2,1)S(1)}, u32[]{:S(2)}, u32[]{:S(2)}) collective-permute-start(bf16[8,512]{1,0:T(8,128)(2,1)S(1)} %get-tuple-element.5), channel_id=1, source_target_pairs={{0,4},{4,8},{8,12},{1,5},{5,9},{9,13},{2,6},{6,10},{10,14},{3,7},{... | collective-permute-start | bytes 24584 | tf_op jit(solution)/shard_map/ppermute | solution.py:18
  228.2 1.3 collective-permute-start.3
  229.5 0.0 collective-permute-done.2
  229.5 4.2 %collective-permute-done.3 = bf16[8,512]{1,0:T(8,128)(2,1)S(1)} collective-permute-done((bf16[8,512]{1,0:T(8,128)(2,1)S(1)}, bf16[8,512]{1,0:T(8,128)(2,1)S(1)}, u32[]{:S(2)}, u32[]{:S(2)}) %collective-permute-start.3) | collective-permute-done | bytes 8224 | tf_op jit(solution)/shard_map/ppermute | solution.py:19
  233.7 1.0 maximum_convert_fusion.1
  234.7 11.3 %convolution_convert_fusion = bf16[384,2048]{1,0:T(8,128)(2,1)} fusion(bf16[2,512,2048]{2,1,0:T(8,128)(2,1)} %all-gather.5.cloned.1.call-done, bf16[2,1,512,512]{3,2,1,0:T(8,128)(2,1)} %param.9, f32[512]{0:T(512)S(1)} %bitcast.86, f32[400,1,512]{2,0,1:T(8,128)} %maximum_convert_fusion.1, f32[384]{0:T(512)S(1)} %subtract_convert_fusion, f32[]{:T(128)S(6)} %mul.373, ...), kind=kOutput, calls=%fused_computation.14 | convolution fusion | flops 1014497280 | bytes 16780864 | tf_op jit(solution)/shard_map/dot_general | solution.py:74
  246.0 0.0 all-reduce.5.cloned.1.call-update
  246.0 42.1 %all-reduce.5.cloned.1.call-done = bf16[384,2048]{1,0:T(8,128)(2,1)} async-done(((bf16[384,2048]{1,0:T(8,128)(2,1)}), bf16[384,2048]{1,0:T(8,128)(2,1)}) %all-reduce.5.cloned.1.call-update) | async-done | bytes 1572880 | tf_op jit(solution)/shard_map/psum | solution.py:75
  288.2 3.4 %fusion.7 = bf16[384,2048]{1,0:T(8,128)(2,1)} fusion(bf16[384,2048]{1,0:T(8,128)(2,1)} %all-reduce.5.cloned.1.call-done, bf16[384,2048]{1,0:T(8,128)(2,1)S(1)} %copy-done.1, bf16[384,2048]{1,0:T(8,128)(2,1)S(1)} %copy-done), kind=kLoop, calls=%fused_computation.13 | loop fusion | flops 6291456 | bytes 6291456 | tf_op jit(solution)/shard_map/convert_element_type | solution.py:76
  (7 shorter events, 0.1 us)
Async XLA Ops:
  6.5 1.5 copy-start
  6.5 1.9 copy-start.3
  6.5 2.0 copy-start.2
  6.5 85.9 %all-gather.3.cloned.1.call-start = ((), (), s32[]{:S(2)}) async-start(), calls=%async_computation | async-start | bytes 5242880 | tf_op jit(solution)/shard_map/all_gather | solution.py:64
  7.3 166.0 %all-gather.5.cloned.1.call-start = ((), (), s32[]{:S(2)}) async-start(), calls=%async_computation.1 | async-start | bytes 5242880 | tf_op jit(solution)/shard_map/all_gather | solution.py:65
  8.0 212.0 %all-reduce.3.cloned.1.call-start = ((), (), s32[]{:S(2)}) async-start(), calls=%async_computation.2 | async-start | bytes 3145728 | tf_op jit(solution)/shard_map/psum | solution.py:75
  95.0 2.7 collective-permute-start
  96.3 5.6 %collective-permute-start.1 = (bf16[8,512]{1,0:T(8,128)(2,1)S(1)}, bf16[8,512]{1,0:T(8,128)(2,1)S(1)}, u32[]{:S(2)}, u32[]{:S(2)}) collective-permute-start(bf16[8,512]{1,0:T(8,128)(2,1)S(1)} %get-tuple-element.8), channel_id=1, source_target_pairs={{4,0},{8,4},{12,8},{5,1},{9,5},{13,9},{6,2},{10,6},{14,10},{7,3},{... | collective-permute-start | bytes 24584 | tf_op jit(solution)/shard_map/ppermute | solution.py:19
  178.5 109.6 %all-reduce.5.cloned.1.call-start = ((), (), s32[]{:S(2)}) async-start(), calls=%async_computation.3 | async-start | bytes 3145728 | tf_op jit(solution)/shard_map/psum | solution.py:75
  220.0 2.1 copy-start.1
  224.8 4.7 %collective-permute-start.2 = (bf16[8,512]{1,0:T(8,128)(2,1)S(1)}, bf16[8,512]{1,0:T(8,128)(2,1)S(1)}, u32[]{:S(2)}, u32[]{:S(2)}) collective-permute-start(bf16[8,512]{1,0:T(8,128)(2,1)S(1)} %get-tuple-element.5), channel_id=1, source_target_pairs={{0,4},{4,8},{8,12},{1,5},{5,9},{9,13},{2,6},{6,10},{10,14},{3,7},{... | collective-permute-start | bytes 24584 | tf_op jit(solution)/shard_map/ppermute | solution.py:18
  228.2 5.5 %collective-permute-start.3 = (bf16[8,512]{1,0:T(8,128)(2,1)S(1)}, bf16[8,512]{1,0:T(8,128)(2,1)S(1)}, u32[]{:S(2)}, u32[]{:S(2)}) collective-permute-start(bf16[8,512]{1,0:T(8,128)(2,1)S(1)} %get-tuple-element.6), channel_id=1, source_target_pairs={{4,0},{8,4},{12,8},{5,1},{9,5},{13,9},{6,2},{10,6},{14,10},{7,3},{... | collective-permute-start | bytes 24584 | tf_op jit(solution)/shard_map/ppermute | solution.py:19
Sparse Core Ops, SparseCore 0:
  8.9 83.4 all-gather.2
  94.0 79.2 all-gather.4
  178.6 41.3 all-reduce.2
  246.1 41.9 all-reduce.4
where the time goes:
time: 298 us
  waiting for transfers between devices  249 us (84%)
  matrix products  21.8 us (7%)
  between operations  13.4 us (4%)
  starting transfers between devices  7.37 us (2%)
  other arithmetic  6.97 us (2%)
    all_gather x1, waiting for transfers between devices, per_device(): lax.all_gather(entry_weight, 'sp', axis=1, tiled=True)  83.9 us
    psum x2, waiting for transfers between devices, per_device(): summed = lax.psum(update.astype(jnp.bfloat16), 'tp').astype(jnp.float32)  83.6 us
    all_gather x1, waiting for transfers between devices, per_device(): lax.all_gather(back_weight, 'sp', axis=2, tiled=True)  71.2 us
    dot_general x2, matrix products, per_device(): update = jnp.dot(mixed, back_local, preferred_element_type=jnp.float32)  16.5 us
    ppermute x2, waiting for transfers between devices, extended_2(): after = lax.ppermute(first, axis, down)  8.37 us
  transfers between devices with their start and end apart: 8, of which 6 were waited for; matrix products, arithmetic and copies ran while one was open for 1% of the time, Pallas kernels for 0%

commit v1 on v0

--- a/solution.py
+++ b/solution.py
@@ -72,7 +72,9 @@
         back_local = back_all[layer]
         mixed = pool_groups(pooled_in, mix_weight[layer], pool_gain[layer], reach)
         update = jnp.dot(mixed, back_local, preferred_element_type=jnp.float32)
-        summed = lax.psum(update.astype(jnp.bfloat16), "tp").astype(jnp.float32)
+        summed = jnp.sum(lax.all_gather(update.astype(jnp.bfloat16), "tp"), axis=0).astype(
+            jnp.float32
+        )
         state = (state.astype(jnp.float32) + summed).astype(jnp.bfloat16)
     return state
 

time: 298 us -> 314 us (1.054)
  other arithmetic: 6.97 us -> 15.3 us
  waiting for transfers between devices: 249 us -> 255 us
    all_gather x0 -> x2, waiting for transfers between devices: none -> 90.5 us  [per_device(): lax.all_gather(update.astype(jnp.bfloat16), 'tp')]
    psum x2 -> x0, waiting for transfers between devices: 83.6 us -> none  [per_device(): summed = lax.psum(update.astype(jnp.bfloat16), 'tp').astype(jnp.float32)]
    reduce_sum x0 -> x2, other arithmetic: none -> 9.86 us  [per_device(): jnp.sum(lax.all_gather(update.astype(jnp.bfloat16), 'tp'), axis=0)]
where the time goes in v1:
time: 314 us; the launch traced here: 313 us
  waiting for transfers between devices  255 us (81%)
  matrix products  21.6 us (7%)
  other arithmetic  15.3 us (5%)
  between operations  13.4 us (4%)
  starting transfers between devices  7.56 us (2%)
    all_gather x2, waiting for transfers between devices, per_device(): lax.all_gather(update.astype(jnp.bfloat16), 'tp')  90.5 us
    all_gather x1, waiting for transfers between devices, per_device(): lax.all_gather(entry_weight, 'sp', axis=1, tiled=True)  83.9 us
    all_gather x1, waiting for transfers between devices, per_device(): lax.all_gather(back_weight, 'sp', axis=2, tiled=True)  71.2 us
    dot_general x2, matrix products, per_device(): update = jnp.dot(mixed, back_local, preferred_element_type=jnp.float32)  16.4 us
    reduce_sum x2, other arithmetic, per_device(): jnp.sum(lax.all_gather(update.astype(jnp.bfloat16), 'tp'), axis=0)  9.86 us
    ppermute x2, waiting for transfers between devices, extended_2(): after = lax.ppermute(first, axis, down)  8.24 us
  transfers between devices with their start and end apart: 8, of which 6 were waited for; matrix products, arithmetic and copies ran while one was open for 1% of the time, Pallas kernels for 0%

profile of v1, /device:TPU:0, one launch (start us, length us, event | category | flops | bytes accessed | tf_op | source)
XLA Modules:
  0.0 313.2 jit_solution(13601813253154652166)
XLA Ops:
  6.5 0.0 copy-start
  6.5 0.0 copy-start.2
  6.5 0.0 copy-start.1
  6.5 0.0 all-gather.7.cloned.1.call-start
  6.5 0.7 all-gather.7.cloned.1.call-update
  7.3 0.0 all-gather.9.cloned.1.call-start
  7.3 0.7 all-gather.9.cloned.1.call-update
  8.0 0.0 all-gather.11.cloned.1.call-start
  8.1 0.0 copy-done
  8.1 0.4 fusion
  8.5 0.0 copy-done.2
  8.5 0.0 copy-done.1
  8.5 83.9 %all-gather.7.cloned.1.call-done = bf16[2,2048,512]{2,1,0:T(8,128)(2,1)} async-done(((bf16[2,512,512]{2,1,0:T(8,128)(2,1)}), bf16[2,2048,512]{2,1,0:T(8,128)(2,1)}) %all-gather.7.cloned.1.call-update) | async-done | bytes 4194320 | tf_op jit(solution)/shard_map/all_gather | solution.py:64
  92.4 2.6 fusion.20
  95.0 1.3 collective-permute-start
  96.3 1.3 collective-permute-start.1
  97.8 0.0 collective-permute-done
  97.8 4.2 %collective-permute-done.1 = bf16[8,512]{1,0:T(8,128)(2,1)S(1)} collective-permute-done((bf16[8,512]{1,0:T(8,128)(2,1)S(1)}, bf16[8,512]{1,0:T(8,128)(2,1)S(1)}, u32[]{:S(2)}, u32[]{:S(2)}) %collective-permute-start.1) | collective-permute-done | bytes 8224 | tf_op jit(solution)/shard_map/ppermute | solution.py:19
  102.0 0.1 maximum_convert_fusion
  102.1 71.2 %all-gather.9.cloned.1.call-done = bf16[2,512,2048]{2,1,0:T(8,128)(2,1)} async-done(((bf16[2,512,512]{2,1,0:T(8,128)(2,1)}), bf16[2,512,2048]{2,1,0:T(8,128)(2,1)}) %all-gather.9.cloned.1.call-update) | async-done | bytes 4194320 | tf_op jit(solution)/shard_map/all_gather | solution.py:65
  173.2 5.2 %convolution_convert_fusion.1 = bf16[384,2048]{1,0:T(8,128)(2,1)} fusion(bf16[2,512,2048]{2,1,0:T(8,128)(2,1)} %all-gather.9.cloned.1.call-done, bf16[2,1,512,512]{3,2,1,0:T(8,128)(2,1)} %param.9, f32[512]{0:T(512)S(1)} %bitcast.91, f32[400,1,512]{2,0,1:T(8,128)S(1)} %maximum_convert_fusion, f32[384]{0:T(512)S(1)} %subtract_convert_fusion, f32[]{:T(128)S(6)} %mul.373, ...), kind=kOutput, calls=%fused_computation.15 | convolution fusion | flops 1014497280 | bytes 16781376 | tf_op jit(solution)/shard_map/dot_general | solution.py:74
  178.5 0.0 all-gather.11.cloned.1.call-update
  178.5 0.0 all-gather.13.cloned.1.call-start
  178.6 44.9 %all-gather.11.cloned.1.call-done = bf16[1536,2048]{1,0:T(8,128)(2,1)} async-done(((bf16[384,2048]{1,0:T(8,128)(2,1)}), bf16[1536,2048]{1,0:T(8,128)(2,1)}) %all-gather.11.cloned.1.call-update) | async-done | bytes 6291472 | tf_op jit(solution)/shard_map/all_gather | solution.py:75
  223.5 4.2 %reduce_sum.43 = bf16[384,2048]{1,0:T(8,128)(2,1)S(1)} reduce(bf16[4,384,2048]{2,1,0:T(8,128)(2,1)} %bitcast.80, bf16[]{:T(256)} %constant.87.clone.1), dimensions={0}, to_apply=%region_1.0 | reduce | flops 2359296 | bytes 7864322 | tf_op jit(solution)/shard_map/reduce_sum | solution.py:75
  227.7 0.6 fusion.4
  228.3 2.6 fusion.23
  230.9 3.4 %collective-permute-start.2 = (bf16[8,512]{1,0:T(8,128)(2,1)S(1)}, bf16[8,512]{1,0:T(8,128)(2,1)S(1)}, u32[]{:S(2)}, u32[]{:S(2)}) collective-permute-start(bf16[8,512]{1,0:T(8,128)(2,1)S(1)} %get-tuple-element.5), channel_id=1, source_target_pairs={{0,4},{4,8},{8,12},{1,5},{5,9},{9,13},{2,6},{6,10},{10,14},{3,7},{... | collective-permute-start | bytes 24584 | tf_op jit(solution)/shard_map/ppermute | solution.py:18
  234.3 1.5 collective-permute-start.3
  235.8 0.0 collective-permute-done.2
  235.8 4.1 %collective-permute-done.3 = bf16[8,512]{1,0:T(8,128)(2,1)S(1)} collective-permute-done((bf16[8,512]{1,0:T(8,128)(2,1)S(1)}, bf16[8,512]{1,0:T(8,128)(2,1)S(1)}, u32[]{:S(2)}, u32[]{:S(2)}) %collective-permute-start.3) | collective-permute-done | bytes 8224 | tf_op jit(solution)/shard_map/ppermute | solution.py:19
  239.9 1.0 maximum_convert_fusion.1
  240.9 11.1 %convolution_convert_fusion = bf16[384,2048]{1,0:T(8,128)(2,1)} fusion(bf16[2,512,2048]{2,1,0:T(8,128)(2,1)} %all-gather.9.cloned.1.call-done, bf16[2,1,512,512]{3,2,1,0:T(8,128)(2,1)} %param.9, f32[512]{0:T(512)S(1)} %bitcast.90, f32[400,1,512]{2,0,1:T(8,128)} %maximum_convert_fusion.1, f32[384]{0:T(512)S(1)} %subtract_convert_fusion, f32[]{:T(128)S(6)} %mul.373, ...), kind=kOutput, calls=%fused_computation.14 | convolution fusion | flops 1014497280 | bytes 16780864 | tf_op jit(solution)/shard_map/dot_general | solution.py:74
  252.0 0.0 all-gather.13.cloned.1.call-update
  252.1 45.6 %all-gather.13.cloned.1.call-done = bf16[1536,2048]{1,0:T(8,128)(2,1)} async-done(((bf16[384,2048]{1,0:T(8,128)(2,1)}), bf16[1536,2048]{1,0:T(8,128)(2,1)}) %all-gather.13.cloned.1.call-update) | async-done | bytes 6291472 | tf_op jit(solution)/shard_map/all_gather | solution.py:75
  297.7 5.7 %reduce_sum.45 = bf16[384,2048]{1,0:T(8,128)(2,1)} reduce(bf16[4,384,2048]{2,1,0:T(8,128)(2,1)} %bitcast.81, bf16[]{:T(256)} %constant.87.clone.1), dimensions={0}, to_apply=%region_3.0 | reduce | flops 2359296 | bytes 7864322 | tf_op jit(solution)/shard_map/reduce_sum | solution.py:75
  303.3 3.4 %fusion.7 = bf16[384,2048]{1,0:T(8,128)(2,1)} fusion(bf16[384,2048]{1,0:T(8,128)(2,1)} %reduce_sum.45, bf16[384,2048]{1,0:T(8,128)(2,1)S(1)} %reduce_sum.43, bf16[384,2048]{1,0:T(8,128)(2,1)S(1)} %copy-done), kind=kLoop, calls=%fused_computation.13 | loop fusion | flops 6291456 | bytes 6291456 | tf_op jit(solution)/shard_map/convert_element_type | solution.py:78
  (7 shorter events, 0.1 us)
Async XLA Ops:
  6.5 1.5 copy-start
  6.5 1.9 copy-start.2
  6.5 2.0 copy-start.1
  6.5 85.9 %all-gather.7.cloned.1.call-start = ((), (), s32[]{:S(2)}) async-start(), calls=%async_computation | async-start | bytes 5242880 | tf_op jit(solution)/shard_map/all_gather | solution.py:64
  7.3 166.0 %all-gather.9.cloned.1.call-start = ((), (), s32[]{:S(2)}) async-start(), calls=%async_computation.1 | async-start | bytes 5242880 | tf_op jit(solution)/shard_map/all_gather | solution.py:65
  8.0 215.5 %all-gather.11.cloned.1.call-start = ((), (), s32[]{:S(2)}) async-start(), calls=%async_computation.2 | async-start | bytes 7864320 | tf_op jit(solution)/shard_map/all_gather | solution.py:75
  95.0 2.7 collective-permute-start
  96.3 5.6 %collective-permute-start.1 = (bf16[8,512]{1,0:T(8,128)(2,1)S(1)}, bf16[8,512]{1,0:T(8,128)(2,1)S(1)}, u32[]{:S(2)}, u32[]{:S(2)}) collective-permute-start(bf16[8,512]{1,0:T(8,128)(2,1)S(1)} %get-tuple-element.8), channel_id=1, source_target_pairs={{4,0},{8,4},{12,8},{5,1},{9,5},{13,9},{6,2},{10,6},{14,10},{7,3},{... | collective-permute-start | bytes 24584 | tf_op jit(solution)/shard_map/ppermute | solution.py:19
  178.5 119.2 %all-gather.13.cloned.1.call-start = ((), (), s32[]{:S(2)}) async-start(), calls=%async_computation.3 | async-start | bytes 7864320 | tf_op jit(solution)/shard_map/all_gather | solution.py:75
  230.9 4.9 %collective-permute-start.2 = (bf16[8,512]{1,0:T(8,128)(2,1)S(1)}, bf16[8,512]{1,0:T(8,128)(2,1)S(1)}, u32[]{:S(2)}, u32[]{:S(2)}) collective-permute-start(bf16[8,512]{1,0:T(8,128)(2,1)S(1)} %get-tuple-element.5), channel_id=1, source_target_pairs={{0,4},{4,8},{8,12},{1,5},{5,9},{9,13},{2,6},{6,10},{10,14},{3,7},{... | collective-permute-start | bytes 24584 | tf_op jit(solution)/shard_map/ppermute | solution.py:18
  234.3 5.5 %collective-permute-start.3 = (bf16[8,512]{1,0:T(8,128)(2,1)S(1)}, bf16[8,512]{1,0:T(8,128)(2,1)S(1)}, u32[]{:S(2)}, u32[]{:S(2)}) collective-permute-start(bf16[8,512]{1,0:T(8,128)(2,1)S(1)} %get-tuple-element.6), channel_id=1, source_target_pairs={{4,0},{8,4},{12,8},{5,1},{9,5},{13,9},{6,2},{10,6},{14,10},{7,3},{... | collective-permute-start | bytes 24584 | tf_op jit(solution)/shard_map/ppermute | solution.py:19
Sparse Core Ops, SparseCore 0:
  8.9 83.4 all-gather.6
  94.0 79.2 all-gather.8
  178.6 44.8 all-gather.10
  252.2 45.4 all-gather.12
